TPU v7x, 32 devices: a whole 2x2x4 slice. The times are simulated.
32 devices in a mesh: gr: 2 (over y), sp: 4 (over z), tp: 4 (over x, core).
Axes of the slice: x: 2, y: 2, z: 4, core: 2. Of those that a mesh axis runs over, the one named last changes fastest.
Arguments:
- tokens: bfloat16 [8, 768, 4096], P('gr', 'sp'), parts along dimension 0, may hold values from -50 to 50
- new_tokens: bfloat16 [8, 4096], P('gr'), parts along dimension 0, may hold values from -6 to 6
- in_gain: float32 [4096], replicated, may hold values from 0.1 to 1.9
- w_forget: bfloat16 [4096, 2048], P(None, 'tp'), may hold values from -0.09375 to 0.09375
- w_value: bfloat16 [4096, 2048], P(None, 'tp'), may hold values from -0.75 to 0.75
- gap: float32 [16, 128], P('tp'), may hold values from 0 to 0.06
- decay_shift: float32 [8, 768, 16], P('gr', 'sp', 'tp'), parts along dimension 0, may hold values from -3 to 0
- query: bfloat16 [8, 16, 128], P('gr', 'tp', 'sp'), parts along dimension 0, may hold values from -6 to 6
- out_gain: float32 [16, 128], P('tp'), may hold values from 0.1 to 1.9
Outputs:
- cache: bfloat16 [8, 16, 128, 128], P('gr', 'tp', 'sp'), parts along dimension 0
- read: float32 [8, 16, 128], P('gr', 'tp'), parts along dimension 0
There are 2 independent parts, one for each index of `gr`. A program takes and returns all parts, laid end to end along the dimension named above; an argument that names none is the same for every part. Nothing has to cross between parts.
All inputs are finite; a program needn't handle non-finite values.
Results may differ from a plain program's by a relative error of at most 0.0065.
Values sent between devices are 32-bit elements; how exact they have to be, the bound alone decides.
A program may use at most 64 MiB of HBM per device.

v0:
```python
import jax
import jax.numpy as jnp
from jax import lax
from jax.sharding import PartitionSpec as P

epsilon = 1e-06


def normalize(row_block, gain_row):
    widened = row_block.astype(jnp.float32)
    scaled = widened * lax.rsqrt(jnp.mean(widened * widened, axis=-1, keepdims=True) + epsilon)
    return (scaled * gain_row).astype(jnp.bfloat16)


def settle(received):
    stacked, block_sums = received
    later_sum = jnp.cumsum(block_sums[::-1], axis=0)[::-1] - block_sums
    return jnp.sum(jnp.exp(later_sum)[..., None] * stacked, axis=0)


def local(tokens, new_tokens, in_gain, w_forget, w_value, gap, decay_shift, query, out_gain):
    seq_count, seg_len, model_width = tokens.shape
    head_count, key_dim = gap.shape
    val_dim = out_gain.shape[1]
    row_count = key_dim // lax.axis_size("sp")
    unit_norm_rows = normalize(tokens.reshape(seq_count * seg_len, model_width), in_gain)
    forget_pre = jnp.dot(unit_norm_rows, w_forget, preferred_element_type=jnp.float32).reshape(
        seq_count, seg_len, head_count, key_dim
    )
    values = jnp.dot(unit_norm_rows, w_value, preferred_element_type=jnp.float32).astype(
        jnp.bfloat16
    )
    values = values.reshape(seq_count, seg_len, head_count, val_dim)
    key_gate = gap * jax.nn.sigmoid(-forget_pre)
    forget_logarithm = jnp.log1p(-key_gate) + decay_shift[:, :, :, None]
    totals = jnp.sum(forget_logarithm, axis=1)
    within = totals[:, None] - jnp.cumsum(forget_logarithm, axis=1)
    weights = (key_gate * jnp.exp(within)).astype(jnp.bfloat16)
    pieces = jnp.einsum("sthi,sthj->shij", weights, values, preferred_element_type=jnp.float32)
    full_state = settle(
        (
            lax.all_to_all(pieces[None], "sp", split_axis=3, concat_axis=0, tiled=True),
            lax.all_to_all(totals[None], "sp", split_axis=3, concat_axis=0, tiled=True),
        )
    )
    cache = full_state.astype(jnp.bfloat16)
    row_start = lax.axis_index("sp") * row_count
    normed_new = normalize(new_tokens, in_gain)
    new_pre = jnp.dot(normed_new, w_forget, preferred_element_type=jnp.float32).reshape(
        seq_count, head_count, key_dim
    )
    new_key = lax.dynamic_slice_in_dim(gap * jax.nn.sigmoid(-new_pre), row_start, row_count, 2)
    new_values = lax.optimization_barrier(
        jnp.dot(normed_new, w_value, preferred_element_type=jnp.float32).astype(jnp.bfloat16)
    )
    new_values = new_values.astype(jnp.float32).reshape(seq_count, head_count, val_dim)
    updated = (1.0 - new_key)[..., None] * full_state + new_key[..., None] * new_values[
        :, :, None, :
    ]
    partial_value = jnp.einsum(
        "shi,shij->shj", query.astype(jnp.float32), updated, precision=lax.Precision.HIGHEST
    )
    read_raw = lax.psum(partial_value, "sp")
    read = (
        read_raw
        * lax.rsqrt(jnp.mean(read_raw * read_raw, axis=-1, keepdims=True) + epsilon)
        * out_gain
    )
    return (cache, read)


def solution(mesh):
    return jax.shard_map(
        local,
        mesh=mesh,
        in_specs=(
            P("gr", "sp", None),
            P("gr", None),
            P(),
            P(None, "tp"),
            P(None, "tp"),
            P("tp", None),
            P("gr", "sp", "tp"),
            P("gr", "tp", "sp"),
            P("tp", None),
        ),
        out_specs=(P("gr", "tp", "sp", None), P("gr", "tp", None)),
        check_vma=False,
    )
```

profile of v0, /device:TPU:0, one launch (start us, length us, event | category | flops | bytes accessed | tf_op | source)
XLA Modules:
  0.0 92.6 jit_solution(18022183195930927783)
XLA Ops:
  0.6 0.0 copy-start
  0.6 0.0 copy-start.7
  0.7 0.0 copy-start.8
  0.7 6.4 %copy.34 = bf16[512,4096]{1,0:T(8,128)(2,1)} copy(bf16[512,4096]{0,1:T(8,128)(2,1)} %bitcast.65) | data formatting | bytes 8388608 | tf_op jit(solution)/shard_map/dot_general | solution.py:27
  7.1 0.0 copy-start.1
  7.1 0.0 copy-start.6
  7.1 4.2 %multiply_reduce_fusion = f32[4,192]{1,0:T(4,128)S(1)} fusion(bf16[4,192,4096]{2,1,0:T(8,128)(2,1)} %param.9), kind=kLoop, calls=%fused_computation.4 | loop fusion | flops 9436416 | bytes 6294528 | tf_op jit(solution)/shard_map/reduce_sum | solution.py:11
  11.3 0.0 copy-done.7
  11.4 0.0 copy-done.8
  11.4 0.3 copy-done.1
  11.7 0.0 copy-done.6
  11.7 6.4 %fusion.15 = (f32[4,128,4,192]{1,3,2,0:T(8,128)S(1)}, f32[4,192,4,128]{3,1,2,0:T(8,128)S(1)}) fusion(f32[4,4,192]{2,1,0:T(4,128)S(1)} %bitcast.79, f32[128,4]{0,1:T(4,128)S(1)} %bitcast.78, bf16[4,128,4096,1]{2,1,0,3:T(8,128)(2,1)} %bitcast.70, f32[4096]{0:T(1024)S(1)} %copy-done.6, f32[4,192]{1,0:T(4,128)S(1)} %add_rsqrt_fusion, ...), kind=kOutput, calls=%fused_computation.19 | convolution fusion | flops 3235774464 | bytes 13665280 | tf_op jit(solution)/shard_map/dot_general | solution.py:27
  18.1 0.0 copy-start.4
  18.1 1.1 %copy-done.4 = f32[4,192,4,128]{3,1,2,0:T(8,128)} copy-done((f32[4,192,4,128]{3,1,2,0:T(8,128)}, f32[4,192,4,128]{3,1,2,0:T(8,128)S(1)}, u32[]{:S(2)}) %copy-start.4) | copy-done | bytes 1572888
  19.3 0.7 add_reduce_fusion
  20.0 0.2 copy.22
  20.2 0.9 reshape.91
  21.0 6.3 %all-to-all-start = ((f32[4,1,512]{2,1,0:T(1,128)}), f32[4,1,512]{2,1,0:T(1,128)S(1)}, u32[]{:S(2)}, u32[]{:S(2)}) async-start(f32[4,1,512]{2,1,0:T(1,128)} %reshape.91), calls=%async_computation | async-start | bytes 16384 | tf_op jit(solution)/shard_map/all_to_all | solution.py:43
  27.4 0.1 rsqrt.29
  27.5 0.2 pad.3
  27.7 0.0 slice-start
  27.7 1.6 %fusion.8 = f32[4,128,4,2,128]{1,3,2,4,0:T(2,128)S(1)} fusion(f32[4,128,4,2,128]{1,4,3,2,0:T(8,128)S(1)} %bitcast.68), kind=kOutput, calls=%fused_computation.10 | output fusion | flops 66584576 | bytes 4194304 | tf_op jit(solution)/shard_map/reduce-window
  29.3 0.0 copy-start.2
  29.3 1.3 %copy-done.2 = f32[4,128,4,2,128]{1,3,2,4,0:T(2,128)} copy-done((f32[4,128,4,2,128]{1,3,2,4,0:T(2,128)}, f32[4,128,4,2,128]{1,3,2,4,0:T(2,128)S(1)}, u32[]{:S(2)}) %copy-start.2) | copy-done | bytes 2097176
  30.7 0.1 reduce-window.9
  30.7 0.0 slice-start.1
  30.8 1.9 %broadcast_add_fusion = f32[4,128,1,8,128]{1,3,2,4,0:T(8,128)S(1)} fusion(f32[4,128,1,8,128]{1,3,2,4,0:T(8,128)} %bitcast.66, f32[4,128,1,8]{1,3,2,0:T(8,128)S(1)} %bitcast.76), kind=kLoop, calls=%fused_computation.29 | loop fusion | flops 524288 | bytes 4210688 | tf_op jit(solution)/shard_map/reduce_window_sum
  32.6 1.7 %copy.24 = f32[4,128,4,2,128]{1,4,3,2,0:T(8,128)} copy(f32[4,128,4,2,128]{1,3,2,4,0:T(2,128)S(1)} %bitcast.67) | data formatting | bytes 4194304 | tf_op jit(solution)/shard_map/reduce_window_sum
  34.4 0.0 slice-done
  34.4 0.0 slice-done.1
  34.4 2.7 %fusion.1 = bf16[768,4096]{1,0:T(8,128)(2,1)S(1)} fusion(f32[4096]{0:T(1024)S(1)} %copy-done.6, f32[768]{0:T(1024)S(1)} %rsqrt.29, bf16[4,192,4096]{2,1,0:T(8,128)(2,1)S(1)} %bitcast.64), kind=kLoop, calls=%fused_computation.2 | loop fusion | flops 12582912 | bytes 12602368 | tf_op jit(solution)/shard_map/convert_element_type | solution.py:12
  37.1 0.0 copy-start.3
  37.1 6.6 %convolution_convert_fusion = bf16[768,512]{1,0:T(8,128)(2,1)} fusion(bf16[768,4096]{1,0:T(8,128)(2,1)S(1)} %fusion.1, bf16[4096,512]{1,0:T(8,128)(2,1)} %param.13), kind=kOutput, calls=%fused_computation.22 | convolution fusion | flops 3221618688 | bytes 11272192 | tf_op jit(solution)/shard_map/dot_general | solution.py:30
  43.8 1.7 %reshape.84 = bf16[4,192,4,128]{3,2,1,0:T(4,128)(2,1)S(1)} reshape(bf16[768,512]{1,0:T(8,128)(2,1)} %convolution_convert_fusion) | data formatting | bytes 1572864 | tf_op jit(solution)/shard_map/reshape | solution.py:33
  45.5 0.0 copy-done.3
  45.5 0.0 copy-start.5
  45.5 2.1 %convolution_bitcast_fusion = f32[1,4,4,128,128]{4,3,2,1,0:T(8,128)S(1)} fusion(f32[4,256,4,128]{3,1,2,0:T(8,128)S(1)} %bitcast.69, f32[4,192,4,128]{3,1,2,0:T(8,128)} %copy-done.4, bf16[4,192,4,128]{3,2,1,0:T(4,128)(2,1)S(1)} %reshape.84, f32[4,4,128]{2,1,0:T(4,128)S(1)} %add_reduce_fusion, f32[4,128]{1,0:T(4,128)S(1)} %copy-done.7), kind=kOutput, calls=%fused_computation.23 | convolution fusion | flops 102236160 | bytes 4990976 | tf_op jit(solution)/shard_map/sthi,sthj->shij/dot_general | solution.py:39
  47.6 0.0 copy-done.5
  47.6 0.1 fusion.26
  47.8 1.7 %copy.26 = f32[1,4,4,128,128]{4,2,1,0,3:T(4,128)} copy(f32[1,4,4,128,128]{4,3,2,1,0:T(8,128)S(1)} %convolution_bitcast_fusion) | data formatting | bytes 2097152 | tf_op jit(solution)/shard_map/broadcast_in_dim | solution.py:42
  49.5 0.0 all-to-all-done
  49.5 5.1 %all-to-all-start.1 = ((f32[1,4,4,128,128]{4,2,1,0,3:T(4,128)}), f32[1,4,4,128,128]{4,2,1,0,3:T(4,128)S(1)}, u32[]{:S(2)}, u32[]{:S(2)}) async-start(f32[1,4,4,128,128]{4,2,1,0,3:T(4,128)} %copy.26), calls=%async_computation.1 | async-start | bytes 2097152 | tf_op jit(solution)/shard_map/all_to_all | solution.py:42
  54.6 2.9 %convolution_convert_fusion.1 = bf16[4,512]{1,0:T(4,128)(2,1)S(1)} fusion(bf16[4096,512]{1,0:T(8,128)(2,1)} %param.13, bf16[4,4096]{1,0:T(4,128)(2,1)S(1)} %copy-done.5, f32[4096]{0:T(1024)S(1)} %copy-done.6, f32[4]{0:T(128)S(1)} %add_rsqrt_fusion.2), kind=kOutput, calls=%fused_computation.27 | convolution fusion | flops 16844800 | bytes 4247568 | tf_op jit(solution)/shard_map/dot_general | solution.py:54
  57.5 2.9 %fusion.19 = f32[4,512]{1,0:T(4,128)S(1)} fusion(bf16[4096,512]{1,0:T(8,128)(2,1)} %param.12, bf16[4,4096]{1,0:T(4,128)(2,1)S(1)} %copy-done.5, f32[4096]{0:T(1024)S(1)} %copy-done.6, f32[4]{0:T(128)S(1)} %add_rsqrt_fusion.2), kind=kOutput, calls=%fused_computation.26 | convolution fusion | flops 16846848 | bytes 4251664 | tf_op jit(solution)/shard_map/dot_general | solution.py:49
  60.4 0.1 constant_dynamic-slice_fusion
  60.4 0.1 broadcast_subtract_fusion
  60.5 0.1 copy.28
  60.6 0.1 copy.27
  60.8 0.5 broadcast.103
  61.3 0.7 reduce.1
  61.9 0.4 reshape.92
  62.3 0.0 copy-start.9
  62.4 0.1 subtract_exponential_fusion
  62.5 17.2 %all-to-all-done.1 = f32[1,4,4,128,128]{4,2,1,0,3:T(4,128)S(1)} async-done(((f32[1,4,4,128,128]{4,2,1,0,3:T(4,128)}), f32[1,4,4,128,128]{4,2,1,0,3:T(4,128)S(1)}, u32[]{:S(2)}, u32[]{:S(2)}) %all-to-all-start.1) | async-done | bytes 1048608 | tf_op jit(solution)/shard_map/all_to_all | solution.py:42
  79.7 0.8 multiply_reduce_fusion.1
  80.5 0.3 multiply_add_fusion
  80.8 0.7 copy.29
  81.5 0.0 copy-done
  81.5 0.3 fusion.24
  81.8 10.0 %psum.7 = f32[4,4,128]{2,1,0:T(4,128)S(1)} all-reduce(f32[4,4,128]{2,1,0:T(4,128)S(1)} %bitcast.77), channel_id=1, replica_groups=mesh['gr'=2,'sp'=4,'tp'=4] {'sp'}, use_global_device_ids=true, to_apply=%region_7.8 | all-reduce | flops 2048 | bytes 16384 | tf_op jit(solution)/shard_map/psum | solution.py:63
  91.8 0.1 multiply_reduce_fusion.2
  91.9 0.0 copy-done.9
  91.9 0.7 multiply_multiply_fusion
  (10 shorter events, 0.1 us)
Async XLA Ops:
  0.6 80.9 %copy-start = (bf16[4,4,32]{2,1,0:T(4,128)(2,1)S(1)}, bf16[4,4,32]{2,1,0:T(4,128)(2,1)}, u32[]{:S(2)}) copy-start(bf16[4,4,32]{2,1,0:T(4,128)(2,1)} %param.16) | copy-start | bytes 3076
  0.6 10.7 %copy-start.7 = (f32[4,128]{1,0:T(4,128)S(1)}, f32[4,128]{1,0:T(4,128)}, u32[]{:S(2)}) copy-start(f32[4,128]{1,0:T(4,128)} %param.14) | copy-start | bytes 6148
  0.7 10.7 %copy-start.8 = (f32[4,192,4]{1,2,0:T(4,128)S(1)}, f32[4,192,4]{1,2,0:T(4,128)}, u32[]{:S(2)}) copy-start(f32[4,192,4]{1,2,0:T(4,128)} %param.15) | copy-start | bytes 36868
  7.1 4.6 %copy-start.1 = (bf16[4,192,4096]{2,1,0:T(8,128)(2,1)S(1)}, bf16[4,192,4096]{2,1,0:T(8,128)(2,1)}, u32[]{:S(2)}) copy-start(bf16[4,192,4096]{2,1,0:T(8,128)(2,1)} %param.9) | copy-start | bytes 18874372
  7.1 4.6 %copy-start.6 = (f32[4096]{0:T(1024)S(1)}, f32[4096]{0:T(1024)}, u32[]{:S(2)}) copy-start(f32[4096]{0:T(1024)} %param.11) | copy-start | bytes 49156
  18.1 1.2 %copy-start.4 = (f32[4,192,4,128]{3,1,2,0:T(8,128)}, f32[4,192,4,128]{3,1,2,0:T(8,128)S(1)}, u32[]{:S(2)}) copy-start(f32[4,192,4,128]{3,1,2,0:T(8,128)S(1)} %get-tuple-element.9) | copy-start | bytes 4718596
  21.0 28.4 %all-to-all-start = ((f32[4,1,512]{2,1,0:T(1,128)}), f32[4,1,512]{2,1,0:T(1,128)S(1)}, u32[]{:S(2)}, u32[]{:S(2)}) async-start(f32[4,1,512]{2,1,0:T(1,128)} %reshape.91), calls=%async_computation | async-start | bytes 16384 | tf_op jit(solution)/shard_map/all_to_all | solution.py:43
  27.7 6.7 %slice-start = ((s8[6291456]{0:T(1024)(128)(4,1)}), s8[2097152]{0:T(1024)(128)(4,1)S(1)}, s32[]{:S(2)}) async-start(s8[6291456]{0:T(1024)(128)(4,1)} %bitcast.63), calls=%async_computation.2 | async-start | bytes 4194304
  29.3 1.4 %copy-start.2 = (f32[4,128,4,2,128]{1,3,2,4,0:T(2,128)}, f32[4,128,4,2,128]{1,3,2,4,0:T(2,128)S(1)}, u32[]{:S(2)}) copy-start(f32[4,128,4,2,128]{1,3,2,4,0:T(2,128)S(1)} %fusion.8) | copy-start | bytes 6291460
  30.7 3.6 %slice-start.1 = ((s8[6291456]{0:T(1024)(128)(4,1)}), s8[4194304]{0:T(1024)(128)(4,1)S(1)}, s32[]{:S(2)}) async-start(s8[6291456]{0:T(1024)(128)(4,1)} %bitcast.63), calls=%async_computation.3 | async-start | bytes 8388608
  37.1 8.4 %copy-start.3 = (f32[4,128,4,2,128]{1,4,3,2,0:T(8,128)S(1)}, f32[4,128,4,2,128]{1,4,3,2,0:T(8,128)}, u32[]{:S(2)}) copy-start(f32[4,128,4,2,128]{1,4,3,2,0:T(8,128)} %copy.24) | copy-start | bytes 6291460
  45.5 2.1 %copy-start.5 = (bf16[4,4096]{1,0:T(4,128)(2,1)S(1)}, bf16[4,4096]{1,0:T(4,128)(2,1)}, u32[]{:S(2)}) copy-start(bf16[4,4096]{1,0:T(4,128)(2,1)} %param.10) | copy-start | bytes 98308
  49.5 30.3 %all-to-all-start.1 = ((f32[1,4,4,128,128]{4,2,1,0,3:T(4,128)}), f32[1,4,4,128,128]{4,2,1,0,3:T(4,128)S(1)}, u32[]{:S(2)}, u32[]{:S(2)}) async-start(f32[1,4,4,128,128]{4,2,1,0,3:T(4,128)} %copy.26), calls=%async_computation.1 | async-start | bytes 2097152 | tf_op jit(solution)/shard_map/all_to_all | solution.py:42
  62.3 29.6 %copy-start.9 = (f32[4,128]{1,0:T(4,128)S(1)}, f32[4,128]{1,0:T(4,128)}, u32[]{:S(2)}) copy-start(f32[4,128]{1,0:T(4,128)} %param.17) | copy-start | bytes 6148
where the time goes:
time: 93.1 us; the launch traced here: 92.6 us
  matrix products  21.2 us (23%)
  local copies, waits for them, and re-layouts  17.7 us (19%)
  waiting for transfers between devices  17.2 us (18%)
  other arithmetic  14.2 us (15%)
  starting transfers between devices  11.4 us (12%)
  blocking collectives  9.98 us (11%)
    all_to_all x1, waiting for transfers between devices, local(): lax.all_to_all(pieces[None], 'sp', split_axis=3, concat_axis=0, tiled=True)  17.2 us
    psum x1, blocking collectives, local(): read_raw = lax.psum(partial_value, 'sp')  9.98 us
    dot_general x1, matrix products, local(): jnp.dot(unit_norm_rows, w_value, preferred_element_type=jnp.float32)  6.62 us
    dot_general x1, local copies, waits for them, and re-layouts, local(): jnp.dot(unit_norm_rows, w_forget, preferred_element_type=jnp.float32)  6.42 us
    dot_general x1, matrix products, local(): jnp.dot(unit_norm_rows, w_forget, preferred_element_type=jnp.float32)  6.41 us
    all_to_all x1, starting transfers between devices, local(): lax.all_to_all(totals[None], 'sp', split_axis=3, concat_axis=0, tiled=True)  6.35 us
    all_to_all x1, starting transfers between devices, local(): lax.all_to_all(pieces[None], 'sp', split_axis=3, concat_axis=0, tiled=True)  5.1 us
    unnamed x27, local copies, waits for them, and re-layouts  4.8 us
  transfers between devices with their start and end apart: 2, of which 1 were waited for; matrix products, arithmetic and copies ran while one was open for 31% of the time, Pallas kernels for 0%

commit v1 on v0

v1 whole, which is shorter than its diff:
```python
import functools

import jax
import jax.numpy as jnp
from jax import lax
from jax.experimental import pallas as pl
from jax.experimental.pallas import tpu as pltpu
from jax.sharding import PartitionSpec as P

epsilon = 1e-06
LAG = 1
ROWS = 16
TOKEN_CUTS = 4
WEIGHT_CUTS = 2
MESH = pl.DeviceIdType.MESH


def normalize(rows, gain):
    wide = rows.astype(jnp.float32)
    scaled = wide * lax.rsqrt(jnp.mean(wide * wide, axis=-1, keepdims=True) + epsilon)
    return (scaled * gain).astype(jnp.bfloat16)


def column(row, size):
    return jnp.broadcast_to(row, (size, size)).T


def kernel(
    tokens, new_tokens, in_gain, w_forget, w_value, gap, shift, query, out_gain,
    cache, read,
    tok_s, w_s, new_s, gain_s, gap_s, shift_s, query_s, og_s,
    normed, later, pieces, grow, grow_t, from_left, from_right,
    total_s, total_out, total_in, act, extra, spread, parts,
    tok_sem, w_sem, small_sem,
    f_send, f_recv, b_send, b_recv, t_send, t_recv, r_send, r_recv,
):
    g = lax.axis_index("sp")
    n = lax.axis_size("sp")
    seqs, seg, width = tok_s.shape
    wide_blocks, _, cols = w_s.shape
    heads, keys = gap_s.shape
    per = heads // wide_blocks
    vals = og_s.shape[1]
    rows = keys // n
    blocks = seqs * wide_blocks
    half = per * keys

    def tok_copy(s, i):
        part = pl.ds(i * (seg // TOKEN_CUTS), seg // TOKEN_CUTS)
        return pltpu.make_async_copy(tokens.at[s, part], tok_s.at[s, part], tok_sem.at[s, i])

    def w_copy(k, which, i):
        part = pl.ds(i * (width // WEIGHT_CUTS), width // WEIGHT_CUTS)
        source = (w_forget, w_value)[which]
        at = pl.multiple_of(k * half, half)
        return pltpu.make_async_copy(
            source.at[part, pl.ds(at, half)],
            w_s.at[k, part, pl.ds(which * half, half)],
            w_sem.at[k, which, i],
        )

    smalls = [
        pltpu.make_async_copy(a, b, small_sem.at[i])
        for i, (a, b) in enumerate(
            (
                (in_gain, gain_s), (gap, gap_s), (shift, shift_s),
                (new_tokens, new_s), (query, query_s), (out_gain, og_s),
            )
        )
    ]
    smalls[0].start()
    for i in range(TOKEN_CUTS):
        tok_copy(0, i).start()
    for k in range(wide_blocks):
        for i in range(WEIGHT_CUTS):
            for which in range(2):
                w_copy(k, which, i).start()
        if k == 0:
            for copy in smalls[1:3]:
                copy.start()
    for s in range(1, seqs):
        for i in range(TOKEN_CUTS):
            tok_copy(s, i).start()
    for copy in smalls[3:]:
        copy.start()

    barrier = pltpu.get_barrier_semaphore()
    for k in range(1, n):
        pl.semaphore_signal(
            barrier, inc=1, device_id={"sp": lax.rem(g + k, n)}, device_id_type=MESH
        )

    place = lax.broadcasted_iota(jnp.int32, (seg, seg), 0)
    other = lax.broadcasted_iota(jnp.int32, (seg, seg), 1)
    later[...] = jnp.where(other > place, 1.0, 0.0).astype(jnp.bfloat16)
    smalls[0].wait()

    right, left = lax.rem(g + 1, n), lax.rem(g + n - 1, n)

    def forward(b, d):
        return pltpu.make_async_remote_copy(
            src_ref=pieces.at[b, d], dst_ref=from_left.at[b, d],
            send_sem=f_send.at[b, d], recv_sem=f_recv.at[b, d],
            device_id={"sp": right}, device_id_type=MESH,
        )

    def backward(b, d):
        return pltpu.make_async_remote_copy(
            src_ref=pieces.at[b, d], dst_ref=from_right.at[b, d],
            send_sem=b_send.at[b, d], recv_sem=b_recv.at[b, d],
            device_id={"sp": left}, device_id_type=MESH,
        )

    def carried(b):
        return pltpu.make_async_remote_copy(
            src_ref=total_out.at[b], dst_ref=total_in.at[b],
            send_sem=t_send.at[b], recv_sem=t_recv.at[b],
            device_id={"sp": left}, device_id_type=MESH,
        )

    def loop(low, high, body):
        lax.fori_loop(low, high, lambda i, c: (body(i), c)[1], 0)

    def scatter(ref, b, j, square):
        for d in range(n):
            ref[b, d, j] = square[d * rows : (d + 1) * rows]

    def compute(b):
        s, k = b // wide_blocks, b % wide_blocks

        @pl.when(k == 0)
        def _():
            for i in range(TOKEN_CUTS):
                tok_copy(s, i).wait()

            def rows_of(i):
                at = pl.ds(pl.multiple_of(i * ROWS, ROWS), ROWS)
                normed[at, :] = normalize(tok_s[s, at, :], gain_s[...])

            loop(0, seg // ROWS, rows_of)

        @pl.when(s == 0)
        def _():
            for i in range(WEIGHT_CUTS):
                for which in range(2):
                    w_copy(k, which, i).wait()

        @pl.when(b == 0)
        def _():
            for copy in smalls[1:3]:
                copy.wait()

        both = jnp.dot(normed[...], w_s[k], preferred_element_type=jnp.float32)
        forget_pre = both[:, :half]
        values = both[:, half:].astype(jnp.bfloat16)
        shifts = shift_s[s]
        lane = lax.broadcasted_iota(jnp.int32, shifts.shape, 1)
        gains, moves = [], []
        for j in range(per):
            gains.append(gap_s[pl.ds(k * per + j, 1), :])
            one = jnp.sum(jnp.where(lane == k * per + j, shifts, 0.0), axis=1, keepdims=True)
            moves.append(jnp.broadcast_to(one, (seg, keys)))
        key_gate = jnp.concatenate(gains, axis=1) * jax.nn.sigmoid(-forget_pre)
        log_forget = jnp.log1p(-key_gate) + jnp.concatenate(moves, axis=1)
        high = log_forget.astype(jnp.bfloat16)
        rest = log_forget - high.astype(jnp.float32)
        mid = rest.astype(jnp.bfloat16)
        low = (rest - mid.astype(jnp.float32)).astype(jnp.bfloat16)
        sums = jnp.dot(
            later[...], jnp.concatenate([high, mid, low], axis=1),
            preferred_element_type=jnp.float32,
        )
        within = sums[:, :half] + (sums[:, half : 2 * half] + sums[:, 2 * half :])
        totals = jnp.sum(log_forget, axis=0, keepdims=True)
        weights = (key_gate * jnp.exp(within)).astype(jnp.bfloat16)
        total_s[b] = totals
        for j in range(per):
            at = slice(j * keys, (j + 1) * keys)
            piece = lax.dot_general(
                weights[:, at], values[:, j * vals : (j + 1) * vals],
                (((0,), (0,)), ((), ())), preferred_element_type=jnp.float32,
            )
            scatter(pieces, b, j, piece)
            scatter(grow, b, j, jnp.exp(column(totals[:, at], keys)))

    def send_first(b):
        @pl.when(g == 0)
        def _():
            loop(0, n - 1, lambda i: forward(b, n - 1 - i).start())

        @pl.when(g == n - 1)
        def _():
            total_out[b] = total_s[b]
            carried(b).start()
            loop(0, n - 1, lambda d: backward(b, d).start())

    def service(b):
        @pl.when(g < n - 1)
        def _():
            carried(b).wait_recv()
            arrived = total_in[b]
            for j in range(per):
                scatter(grow_t, b, j, jnp.exp(column(arrived[:, j * keys : (j + 1) * keys], keys)))

        @pl.when((g > 0) & (g < n - 1))
        def _():
            total_out[b] = total_in[b] + total_s[b]
            carried(b).start()

            def on_right(i):
                d = n - 1 - i
                forward(b, d).wait_recv()
                pieces[b, d] = grow[b, d] * from_left[b, d] + pieces[b, d]
                forward(b, d).start()

            def on_left(d):
                backward(b, d).wait_recv()
                pieces[b, d] = from_right[b, d] + grow_t[b, d] * pieces[b, d]
                backward(b, d).start()

            loop(0, n - 1 - g, on_right)
            loop(0, g, on_left)

    def step(b):
        compute(b)

        @pl.when(b == 0)
        def _():
            pl.semaphore_wait(barrier, n - 1)

        send_first(b)

        @pl.when(b >= LAG)
        def _():
            service(b - LAG)

    loop(0, blocks, step)
    for b in range(blocks - LAG, blocks):
        service(b)

    for copy in smalls[3:]:
        copy.wait()
    new_normed = normalize(new_s[...], gain_s[...])
    new_normed = jnp.concatenate(
        [new_normed, jnp.zeros((16 - seqs, width), jnp.bfloat16)], axis=0
    ) if seqs < 16 else new_normed
    pick = (
        lax.broadcasted_iota(jnp.int32, (rows, keys), 1)
        == lax.broadcasted_iota(jnp.int32, (rows, keys), 0) + g * rows
    )
    pick = jnp.where(pick, 1.0, 0.0).astype(jnp.bfloat16)
    placed = [
        jnp.dot(query_s[s], pick, preferred_element_type=jnp.float32) for s in range(seqs)
    ]
    for k in range(wide_blocks):
        both = jnp.dot(new_normed, w_s[k], preferred_element_type=jnp.float32)
        for j in range(per):
            h = k * per + j
            new_key = gap_s[h : h + 1, :] * jax.nn.sigmoid(-both[:seqs, j * keys : (j + 1) * keys])
            new_value = both[:seqs, half + j * vals : half + (j + 1) * vals]
            new_value = new_value.astype(jnp.bfloat16).astype(jnp.float32)
            for s in range(seqs):
                q = placed[s][h : h + 1, :]
                key_row = new_key[s : s + 1, :]
                square = column(q * (1.0 - key_row), keys)
                for d in range(n):
                    spread[d] = square[d * rows : (d + 1) * rows]
                b = s * wide_blocks + k
                act[b, j] = spread[g]
                weight = jnp.sum(q * key_row, axis=1, keepdims=True)
                extra[b * per + j : b * per + j + 1, :] = weight * new_value[s : s + 1, :]

    def finish(b):
        @pl.when(g > 0)
        def _():
            forward(b, g).wait_recv()
            pieces[b, g] = pieces[b, g] + grow[b, g] * from_left[b, g]

        @pl.when(g < n - 1)
        def _():
            backward(b, g).wait_recv()
            pieces[b, g] = from_right[b, g] + grow_t[b, g] * pieces[b, g]

    for b in range(blocks):
        finish(b)
        s, k = b // wide_blocks, b % wide_blocks
        for j in range(per):
            state = pieces[b, g, j]
            cache[s, k * per + j] = state.astype(jnp.bfloat16)
            at = b * per + j
            parts[g, at : at + 1, :] = (
                jnp.sum(act[b, j] * state, axis=0, keepdims=True) + extra[at : at + 1, :]
            )

    def share(k):
        to = lax.rem(g + k, n)
        return pltpu.make_async_remote_copy(
            src_ref=parts.at[g], dst_ref=parts.at[g],
            send_sem=r_send.at[k], recv_sem=r_recv.at[k],
            device_id={"sp": to}, device_id_type=MESH,
        )

    def arrival(k):
        source = lax.rem(g + n - k, n)
        return pltpu.make_async_remote_copy(
            src_ref=parts.at[source], dst_ref=parts.at[source],
            send_sem=r_send.at[k], recv_sem=r_recv.at[k],
            device_id={"sp": source}, device_id_type=MESH,
        )

    loop(1, n, lambda k: share(k).start())

    def drain(b):
        @pl.when(g < n - 1)
        def _():
            loop(g + 1, n, lambda d: forward(b, d).wait_send())

        @pl.when(g > 0)
        def _():
            carried(b).wait_send()
            loop(0, g, lambda d: backward(b, d).wait_send())

    loop(0, blocks, drain)
    loop(1, n, lambda k: arrival(k).wait_recv())
    raw = parts[0]
    for d in range(1, n):
        raw = raw + parts[d]
    scaled = raw * lax.rsqrt(jnp.mean(raw * raw, axis=-1, keepdims=True) + epsilon)
    for s in range(seqs):
        read[s] = scaled[s * heads : (s + 1) * heads] * og_s[...]
    loop(1, n, lambda k: share(k).wait_send())


def local(tokens, new_tokens, in_gain, w_forget, w_value, gap, decay_shift, query, out_gain):
    seqs, seg, width = tokens.shape
    heads, keys = gap.shape
    vals = out_gain.shape[1]
    n = lax.axis_size("sp")
    rows = keys // n
    per = 2 if heads % 2 == 0 else 1
    wide_blocks = heads // per
    blocks = seqs * wide_blocks
    f32, bf16 = jnp.float32, jnp.bfloat16
    dma = pltpu.SemaphoreType.DMA
    grid = (blocks, n, per, rows, vals)
    return pl.pallas_call(
        kernel,
        out_shape=(
            jax.ShapeDtypeStruct((seqs, heads, rows, vals), bf16),
            jax.ShapeDtypeStruct((seqs, heads, vals), f32),
        ),
        in_specs=[pl.BlockSpec(memory_space=pl.ANY)] * 9,
        out_specs=(pl.BlockSpec(memory_space=pltpu.VMEM),) * 2,
        scratch_shapes=[
            pltpu.VMEM((seqs, seg, width), bf16),
            pltpu.VMEM((wide_blocks, width, per * (keys + vals)), bf16),
            pltpu.VMEM((seqs, width), bf16),
            pltpu.VMEM((1, width), f32),
            pltpu.VMEM((heads, keys), f32),
            pltpu.VMEM((seqs, seg, heads), f32),
            pltpu.VMEM((seqs, heads, rows), bf16),
            pltpu.VMEM((heads, vals), f32),
            pltpu.VMEM((seg, width), bf16),
            pltpu.VMEM((seg, seg), bf16),
            pltpu.VMEM(grid, f32),
            pltpu.VMEM(grid, f32),
            pltpu.VMEM(grid, f32),
            pltpu.VMEM(grid, f32),
            pltpu.VMEM(grid, f32),
            pltpu.VMEM((blocks, 1, per * keys), f32),
            pltpu.VMEM((blocks, 1, per * keys), f32),
            pltpu.VMEM((blocks, 1, per * keys), f32),
            pltpu.VMEM((blocks, per, rows, vals), f32),
            pltpu.VMEM((blocks * per, vals), f32),
            pltpu.VMEM((n, rows, vals), f32),
            pltpu.VMEM((n, blocks * per, vals), f32),
            dma((seqs, TOKEN_CUTS)),
            dma((wide_blocks, 2, WEIGHT_CUTS)),
            dma((6,)),
            dma((blocks, n)),
            dma((blocks, n)),
            dma((blocks, n)),
            dma((blocks, n)),
            dma((blocks,)),
            dma((blocks,)),
            dma((n,)),
            dma((n,)),
        ],
        compiler_params=pltpu.CompilerParams(
            collective_id=0, has_side_effects=True, vmem_limit_bytes=60 * 1024 * 1024
        ),
        name="recurrence",
    )(
        tokens, new_tokens, in_gain.reshape(1, width), w_forget, w_value, gap,
        decay_shift, query, out_gain,
    )


def solution(mesh):
    return jax.shard_map(
        local,
        mesh=mesh,
        in_specs=(
            P("gr", "sp", None),
            P("gr", None),
            P(),
            P(None, "tp"),
            P(None, "tp"),
            P("tp", None),
            P("gr", "sp", "tp"),
            P("gr", "tp", "sp"),
            P("tp", None),
        ),
        out_specs=(P("gr", "tp", "sp", None), P("gr", "tp", None)),
        check_vma=False,
    )
```

time: 93.1 us -> 90.2 us (0.969)
  Pallas kernels: 0 us -> 84.7 us
  matrix products: 21.2 us -> 0 us
  waiting for transfers between devices: 17.2 us -> 0 us
  other arithmetic: 14.2 us -> 0 us
  local copies, waits for them, and re-layouts: 17.7 us -> 4.51 us
  starting transfers between devices: 11.4 us -> 0 us
  blocking collectives: 9.98 us -> 0 us
    pallas_call x0 -> x1, Pallas kernels: none -> 84.7 us  [local(): pl.pallas_call(kernel, out_shape=(jax.ShapeDtypeStruct((seqs, heads, rows...]
    dot_general x6 -> x0, matrix products: 21.2 us -> none  [the longest x1 6.62 us: local(): jnp.dot(unit_norm_rows, w_value, preferred_element_type=jnp.float32)]
    all_to_all x2 -> x0, waiting for transfers between devices: 17.2 us -> none  [the longest x1 17.2 us: local(): lax.all_to_all(pieces[None], 'sp', split_axis=3, concat_axis=0, tiled=True)]
    all_to_all x2 -> x0, starting transfers between devices: 11.4 us -> none  [the longest x1 6.35 us: local(): lax.all_to_all(totals[None], 'sp', split_axis=3, concat_axis=0, tiled=True)]
    psum x1 -> x0, blocking collectives: 9.98 us -> none  [local(): read_raw = lax.psum(partial_value, 'sp')]
    dot_general x1 -> x0, local copies, waits for them, and re-layouts: 6.42 us -> none  [local(): jnp.dot(unit_norm_rows, w_forget, preferred_element_type=jnp.float32)]
    reduce_sum x5 -> x0, other arithmetic: 5.96 us -> none  [the longest x2 4.39 us: normalize(): jnp.mean(widened * widened, axis=-1, keepdims=True) + epsilon]
    another operation x4 -> x0, other arithmetic: 3.6 us -> none
  transfers between devices with their start and end apart: 2 -> 0, of which waited for: 1 -> 0; matrix products, arithmetic and copies ran while one was open for 31% -> 0% of each run, Pallas kernels for 0% -> 0%
where the time goes in v1:
time: 90.2 us; the launch traced here: 89.9 us
  Pallas kernels  84.7 us (94%)
  local copies, waits for them, and re-layouts  4.51 us (5%)
    pallas_call x1, Pallas kernels, local(): pl.pallas_call(kernel, out_shape=(jax.ShapeDtypeStruct((seqs, heads, rows...  84.7 us
    unnamed x3, local copies, waits for them, and re-layouts  4.51 us

profile of v1, /device:TPU:0, one launch (start us, length us, event | category | flops | bytes accessed | tf_op | source)
XLA Modules:
  0.0 89.9 jit_solution(13102542166623721743)
XLA Ops:
  0.6 1.6 %copy.11.shift = f32[4,192,4]{2,1,0:T(8,128)} copy(f32[4,192,4]{1,2,0:T(4,128)} %param.15) | data formatting | bytes 24576 | tf_op args[6]
  2.3 84.7 %recurrence.1 = (bf16[4,4,32,128]{3,2,1,0:T(8,128)(2,1)}, f32[4,4,128]{2,1,0:T(4,128)}) custom-call(bf16[4,192,4096]{2,1,0:T(8,128)(2,1)} %tokens.1, bf16[4,4096]{1,0:T(4,128)(2,1)} %new_tokens.1, f32[1,4096]{1,0:T(1,128)} %bitcast.1, bf16[4096,512]{1,0:T(8,128)(2,1)} %w_forget.1, bf16[4096,512]{1,0:T(8,128)(2,1)} %w_value.1, f32[4,128]{1,0:T(4,128)} %gap.1, ...), custom_call_target="tpu_custom_call" | custom-call | tf_op jit(solution)/shard_map/recurrence/pallas_call | solution.py:346
  87.0 1.6 %copy.14 = bf16[4,4,32,128]{3,2,1,0:T(8,128)(2,1)} copy(bf16[4,4,32,128]{3,2,1,0:T(8,128)(2,1)} %get-tuple-element.4) | data formatting | bytes 262144
  88.6 1.3 %copy.15 = f32[4,4,128]{2,1,0:T(4,128)} copy(f32[4,4,128]{2,1,0:T(4,128)} %get-tuple-element.5) | data formatting | bytes 16384

commit v2 on v1

--- a/solution.py
+++ b/solution.py
@@ -8,7 +8,6 @@
 from jax.sharding import PartitionSpec as P
 
 epsilon = 1e-06
-LAG = 1
 ROWS = 16
 TOKEN_CUTS = 4
 WEIGHT_CUTS = 2
@@ -153,15 +152,17 @@
         both = jnp.dot(normed[...], w_s[k], preferred_element_type=jnp.float32)
         forget_pre = both[:, :half]
         values = both[:, half:].astype(jnp.bfloat16)
-        shifts = shift_s[s]
-        lane = lax.broadcasted_iota(jnp.int32, shifts.shape, 1)
-        gains, moves = [], []
-        for j in range(per):
-            gains.append(gap_s[pl.ds(k * per + j, 1), :])
-            one = jnp.sum(jnp.where(lane == k * per + j, shifts, 0.0), axis=1, keepdims=True)
-            moves.append(jnp.broadcast_to(one, (seg, keys)))
+        chosen = (
+            lax.broadcasted_iota(jnp.int32, (heads, half), 0)
+            == lax.broadcasted_iota(jnp.int32, (heads, half), 1) // keys + k * per
+        )
+        moves = lax.dot_general(
+            shift_s[s], jnp.where(chosen, 1.0, 0.0), (((0,), (0,)), ((), ())),
+            precision=lax.Precision.HIGHEST, preferred_element_type=jnp.float32,
+        )
+        gains = [gap_s[pl.ds(k * per + j, 1), :] for j in range(per)]
         key_gate = jnp.concatenate(gains, axis=1) * jax.nn.sigmoid(-forget_pre)
-        log_forget = jnp.log1p(-key_gate) + jnp.concatenate(moves, axis=1)
+        log_forget = jnp.log1p(-key_gate) + moves
         high = log_forget.astype(jnp.bfloat16)
         rest = log_forget - high.astype(jnp.float32)
         mid = rest.astype(jnp.bfloat16)
@@ -194,32 +195,43 @@
             carried(b).start()
             loop(0, n - 1, lambda d: backward(b, d).start())
 
-    def service(b):
-        @pl.when(g < n - 1)
-        def _():
-            carried(b).wait_recv()
-            arrived = total_in[b]
-            for j in range(per):
-                scatter(grow_t, b, j, jnp.exp(column(arrived[:, j * keys : (j + 1) * keys], keys)))
-
-        @pl.when((g > 0) & (g < n - 1))
+    def to_right(b):
+        def each(i):
+            d = n - 1 - i
+            forward(b, d).wait_recv()
+            pieces[b, d] = grow[b, d] * from_left[b, d] + pieces[b, d]
+            forward(b, d).start()
+
+        loop(0, n - 1 - g, each)
+
+    def to_left(b):
+        carried(b).wait_recv()
+        arrived = total_in[b]
+        for j in range(per):
+            scatter(grow_t, b, j, jnp.exp(column(arrived[:, j * keys : (j + 1) * keys], keys)))
+
+        def each(d):
+            backward(b, d).wait_recv()
+            pieces[b, d] = from_right[b, d] + grow_t[b, d] * pieces[b, d]
+            backward(b, d).start()
+
+        @pl.when(g > 0)
         def _():
             total_out[b] = total_in[b] + total_s[b]
             carried(b).start()
-
-            def on_right(i):
-                d = n - 1 - i
-                forward(b, d).wait_recv()
-                pieces[b, d] = grow[b, d] * from_left[b, d] + pieces[b, d]
-                forward(b, d).start()
-
-            def on_left(d):
-                backward(b, d).wait_recv()
-                pieces[b, d] = from_right[b, d] + grow_t[b, d] * pieces[b, d]
-                backward(b, d).start()
-
-            loop(0, n - 1 - g, on_right)
-            loop(0, g, on_left)
+            loop(0, g, each)
+
+    def serve(t):
+        right_b = t - g - 1
+        left_b = t - n + g
+
+        @pl.when((g > 0) & (g < n - 1) & (right_b >= 0) & (right_b < blocks))
+        def _():
+            to_right(right_b)
+
+        @pl.when((g < n - 1) & (left_b >= 0) & (left_b < blocks))
+        def _():
+            to_left(left_b)
 
     def step(b):
         compute(b)
@@ -229,15 +241,10 @@
             pl.semaphore_wait(barrier, n - 1)
 
         send_first(b)
-
-        @pl.when(b >= LAG)
-        def _():
-            service(b - LAG)
+        serve(b)
 
     loop(0, blocks, step)
-    for b in range(blocks - LAG, blocks):
-        service(b)
-
+    serve(blocks)
     for copy in smalls[3:]:
         copy.wait()
     new_normed = normalize(new_s[...], gain_s[...])
@@ -270,6 +277,8 @@
                 weight = jnp.sum(q * key_row, axis=1, keepdims=True)
                 extra[b * per + j : b * per + j + 1, :] = weight * new_value[s : s + 1, :]
 
+    loop(blocks + 1, blocks + n, serve)
+
     def finish(b):
         @pl.when(g > 0)
         def _():
@@ -357,7 +366,7 @@
             pltpu.VMEM((seqs, width), bf16),
             pltpu.VMEM((1, width), f32),
             pltpu.VMEM((heads, keys), f32),
-            pltpu.VMEM((seqs, seg, heads), f32),
+            pltpu.VMEM((seqs, heads, seg), f32),
             pltpu.VMEM((seqs, heads, rows), bf16),
             pltpu.VMEM((heads, vals), f32),
             pltpu.VMEM((seg, width), bf16),
@@ -392,7 +401,7 @@
         name="recurrence",
     )(
         tokens, new_tokens, in_gain.reshape(1, width), w_forget, w_value, gap,
-        decay_shift, query, out_gain,
+        decay_shift.transpose(0, 2, 1), query, out_gain,
     )
 
 

time: 90.2 us -> 50.6 us (0.56)
  Pallas kernels: 84.7 us -> 46.9 us
  local copies, waits for them, and re-layouts: 4.51 us -> 2.86 us
    pallas_call x1, Pallas kernels: 84.7 us -> 46.9 us  [local(): pl.pallas_call(kernel, out_shape=(jax.ShapeDtypeStruct((seqs, heads, rows...]
    unnamed x3 -> x2, local copies, waits for them, and re-layouts: 4.51 us -> 2.86 us
where the time goes in v2:
time: 50.6 us; the launch traced here: 50.4 us
  Pallas kernels  46.9 us (93%)
  local copies, waits for them, and re-layouts  2.86 us (6%)
  between operations  0.64 us (1%)
    pallas_call x1, Pallas kernels, local(): pl.pallas_call(kernel, out_shape=(jax.ShapeDtypeStruct((seqs, heads, rows...  46.9 us
    unnamed x2, local copies, waits for them, and re-layouts  2.86 us

profile of v2, /device:TPU:0, one launch (start us, length us, event | category | flops | bytes accessed | tf_op | source)
XLA Modules:
  0.0 50.4 jit_solution(16235570124566031472)
XLA Ops:
  0.6 46.9 %recurrence.1 = (bf16[4,4,32,128]{3,2,1,0:T(8,128)(2,1)}, f32[4,4,128]{2,1,0:T(4,128)}) custom-call(bf16[4,192,4096]{2,1,0:T(8,128)(2,1)} %tokens.1, bf16[4,4096]{1,0:T(4,128)(2,1)} %new_tokens.1, f32[1,4096]{1,0:T(1,128)} %bitcast.2, bf16[4096,512]{1,0:T(8,128)(2,1)} %w_forget.1, bf16[4096,512]{1,0:T(8,128)(2,1)} %w_value.1, f32[4,128]{1,0:T(4,128)} %gap.1, ...), custom_call_target="tpu_custom_call" | custom-call | tf_op jit(solution)/shard_map/recurrence/pallas_call | solution.py:355
  47.5 1.6 %copy.13 = bf16[4,4,32,128]{3,2,1,0:T(8,128)(2,1)} copy(bf16[4,4,32,128]{3,2,1,0:T(8,128)(2,1)} %get-tuple-element.4) | data formatting | bytes 262144
  49.1 1.3 %copy.14 = f32[4,4,128]{2,1,0:T(4,128)} copy(f32[4,4,128]{2,1,0:T(4,128)} %get-tuple-element.5) | data formatting | bytes 16384
